TPU v7x, 512 devices: a whole 4x4x16 slice. The times are simulated.
512 devices in a mesh: ep: 128 (over z, x, core), tp: 4 (over y).
Axes of the slice: x: 4, y: 4, z: 16, core: 2. Of those that a mesh axis runs over, the one named last changes fastest.
Arguments:
- tokens: bfloat16 [3072, 2048], P('ep'), may hold values from -24 to 24
- carried_state: float32 [3072, 4, 128, 128], P('ep', 'tp'), may hold values from -4 to 4
- w_query: bfloat16 [2048, 512], P(None, 'tp'), may hold values from -0.125 to 0.125
- w_forget: bfloat16 [2048, 512], P(None, 'tp'), may hold values from -0.125 to 0.125
- w_value: bfloat16 [2048, 512], P(None, 'tp'), may hold values from -0.125 to 0.125
- forget_floor: float32 [4, 128], P('tp'), may hold values from 0.05 to 0.9
- head_gain: bfloat16 [4, 128], P('tp'), may hold values from 0.099609375 to 1.8984375
- w_out: bfloat16 [512, 2048], P('tp', 'ep'), may hold values from -0.25 to 0.25
- gain_mix: bfloat16 [2048], replicated, may hold values from 0.099609375 to 1.8984375
- gain_ffn: bfloat16 [2048], replicated, may hold values from 0.099609375 to 1.8984375
- gain_post: bfloat16 [2048], P('tp'), may hold values from 0.099609375 to 1.8984375
- w_branch_gate: bfloat16 [2048], replicated, may hold values from -0.125 to 0.125
- shared_gate: bfloat16 [2048, 512], P('ep', 'tp'), may hold values from -0.125 to 0.125
- shared_up: bfloat16 [2048, 512], P('ep', 'tp'), may hold values from -0.125 to 0.125
- shared_down: bfloat16 [512, 2048], P('tp', 'ep'), may hold values from -1.1048543 to 1.1048543
- routes: int32 [3072, 6], P('ep'), may hold values from 0 to 127, all different within a row; in each aligned block of 24 rows (0 to 23, 24 to 47, ...) at most 2 rows name the same one
- route_weights: float32 [3072, 6], P('ep'), may hold values from 0.2 to 1
- expert_gate: bfloat16 [128, 2048, 512], P('ep', None, 'tp'), may hold values from -0.125 to 0.125
- expert_up: bfloat16 [128, 2048, 512], P('ep', None, 'tp'), may hold values from -0.125 to 0.125
- expert_down: bfloat16 [128, 512, 2048], P('ep', 'tp'), may hold values from -1.1048543 to 1.1048543
Outputs:
- layer_out: bfloat16 [3072, 2048], P('ep', 'tp')
- new_state: float32 [3072, 4, 128, 128], P('ep', 'tp')
Inputs may be any that keep to these rules, and one draw needn't show every extreme that they name: `routes`: among the 24 rows of one index of ep, no expert is named by more than 2 rows, a bound that some block reaches.
All inputs are finite; a program needn't handle non-finite values.
Results may differ from a plain program's by a relative error of at most 0.015.
Values may be sent and summed in bfloat16 or wider, within the bound.
No kernel may reach another device: no remote copies, remote signals or barrier semaphores. Data moves between devices by JAX's collectives and lax.ppermute only.
A program may use at most 64 MiB of HBM per device.

v0:
```python
import jax
import jax.numpy as jnp
from jax import lax
from jax.sharding import Mesh
from jax.sharding import PartitionSpec as P

EP = ("ep_0", "ep_1", "ep_2")


epsilon = 1e-06


def laid_out(parts, dim):
    shape = list(parts.shape[1:])
    shape[dim] *= parts.shape[0]
    return jnp.moveaxis(parts, 0, dim).reshape(shape)


def gather_in_order(value, axes, sequence):
    parts = value
    for k in sequence:
        parts = lax.all_gather(parts, axes[k])
    done = sequence[::-1]
    back = [done.index(k) for k in range(len(axes))]
    parts = parts.transpose(*back, *range(len(axes), parts.ndim))
    return parts.reshape(-1, *value.shape)


def gathered_by_axis(value, axes, sequence, dim):
    return laid_out(gather_in_order(value, axes, sequence), dim)


def sent_to_all(value, axis):
    devices = lax.axis_size(axis)
    return lax.all_to_all(
        jnp.broadcast_to(value[None], (devices, *value.shape)), axis, 0, 0, tiled=True
    )


def taken_together(value, axis):
    return sent_to_all(value, axis).astype(jnp.float32).sum(axis=0)


def sent_together(arrays, axis, dim, along):
    ends, at = ([], 0)
    for a in arrays[:-1]:
        at += a.shape[along]
        ends.append(at)
    both = jnp.concatenate(arrays, axis=along)
    return tuple(jnp.split(lax.all_gather(both, axis, axis=dim, tiled=True), ends, axis=along))


def in_blocks(value, dim, devices):
    before, after = (value.shape[:dim], value.shape[dim + 1 :])
    return jnp.moveaxis(value.reshape(*before, devices, -1, *after), dim, 0)


def sent_and_summed(value, axis, dim):
    devices = lax.axis_size(axis)
    parts = lax.all_to_all(in_blocks(value, dim, devices), axis, 0, 0, tiled=True)
    return jnp.sum(parts.astype(jnp.float32), axis=0)


def taken_together_2(value, axis):
    everything = sent_to_all(value, axis)
    return jnp.sum(everything, axis=0)


def rmsnorm(values_in, gain):
    scale = lax.rsqrt(jnp.mean(values_in * values_in, axis=-1, keepdims=True) + epsilon)
    return values_in * scale * gain.astype(jnp.float32)


def project_down(acts, weight):
    projected = jnp.dot(
        acts, gathered_by_axis(weight, EP, (1, 0, 2), 1), preferred_element_type=jnp.float32
    )
    return projected.astype(jnp.bfloat16)


def shards(
    tokens,
    carried_state,
    w_query,
    w_forget,
    w_value,
    forget_floor,
    head_gain,
    w_out,
    gain_mix,
    gain_ffn,
    gain_post,
    w_branch_gate,
    shared_gate,
    shared_up,
    shared_down,
    routes,
    route_weights,
    expert_gate,
    expert_up,
    expert_down,
):
    seq_rows, model_width = tokens.shape
    heads_local = carried_state.shape[1]
    head_dim = carried_state.shape[2]
    n_ep = lax.axis_size(EP)
    n_tp = lax.axis_size("tp")
    top_count = routes.shape[1]
    experts_local = expert_gate.shape[0]
    experts_all = experts_local * n_ep
    capacity = min(
        seq_rows, max(2, (3 * seq_rows * top_count + 2 * experts_all - 1) // (2 * experts_all))
    )
    slice_width = model_width // n_tp
    normed = rmsnorm(tokens.astype(jnp.float32), gain_mix).astype(jnp.bfloat16)
    queries = jax.nn.silu(jnp.dot(normed, w_query, preferred_element_type=jnp.float32))
    forget_pre = jnp.dot(normed, w_forget, preferred_element_type=jnp.float32)
    values_in = jnp.dot(normed, w_value, preferred_element_type=jnp.float32)
    queries = queries.reshape(seq_rows, heads_local, head_dim)
    forget_pre = forget_pre.reshape(seq_rows, heads_local, head_dim)
    values_in = values_in.reshape(seq_rows, heads_local, head_dim)
    forget = forget_floor + (1.0 - forget_floor) * jax.nn.sigmoid(forget_pre)
    keys_in = (1.0 - forget_floor) * jax.nn.sigmoid(-forget_pre)
    new_state = forget[..., None] * carried_state + keys_in[..., None] * values_in[:, :, None, :]
    readout = jnp.einsum("bhd,bhdv->bhv", queries, new_state, precision=lax.Precision.HIGHEST)
    head_out = (
        rmsnorm(readout, head_gain).astype(jnp.bfloat16).reshape(seq_rows, heads_local * head_dim)
    )
    head_terms = project_down(head_out, w_out)
    mixed = (
        taken_together(head_terms.astype(jnp.float32).astype(jnp.bfloat16), "tp")
        .astype(jnp.float32)
        .astype(jnp.bfloat16)
    )
    resid = (tokens.astype(jnp.float32) + mixed.astype(jnp.float32)).astype(jnp.bfloat16)
    hnorm = rmsnorm(resid.astype(jnp.float32), gain_ffn).astype(jnp.bfloat16)
    branch_mix = jax.nn.sigmoid(jnp.dot(hnorm, w_branch_gate, preferred_element_type=jnp.float32))
    pieces = sent_together((shared_gate, shared_up), EP, 0, 1)
    gate_pre = jnp.dot(hnorm, pieces[0], preferred_element_type=jnp.float32)
    up_pre = jnp.dot(hnorm, pieces[1], preferred_element_type=jnp.float32)
    shared_hidden = (jax.nn.silu(gate_pre) * up_pre).astype(jnp.bfloat16)
    shared_terms = project_down(shared_hidden, shared_down)
    shared_out = sent_and_summed(
        shared_terms.astype(jnp.float32).astype(jnp.bfloat16), "tp", 1
    ).astype(jnp.bfloat16)
    flat_routes = routes.reshape(-1)
    expert_ids = lax.broadcasted_iota(jnp.int32, (1, experts_all), 1)
    onehot = (flat_routes[:, None] == expert_ids).astype(jnp.int32)
    earlier = jnp.cumsum(onehot, axis=0) - onehot
    slot_rank = jnp.sum(earlier * onehot, axis=1)
    position = flat_routes * capacity + slot_rank
    slot_ids = lax.broadcasted_iota(jnp.int32, (1, experts_all * capacity), 1)
    slot_match = position[:, None] == slot_ids
    repeated = jnp.repeat(hnorm, top_count, axis=0)
    send_rows = jnp.einsum(
        "rs,rd->sd", slot_match.astype(jnp.bfloat16), repeated, preferred_element_type=jnp.float32
    )
    send_rows = send_rows.astype(jnp.bfloat16).reshape(experts_all, capacity, model_width)
    arrived = lax.all_to_all(send_rows, EP, split_axis=0, concat_axis=0, tiled=True)
    slot_count = arrived.shape[1]
    slotted = arrived.reshape(n_ep, experts_local, slot_count, model_width)
    expert_gate_pre = jnp.einsum(
        "sxnd,xdf->sxnf", slotted, expert_gate, preferred_element_type=jnp.float32
    )
    expert_up_pre = jnp.einsum(
        "sxnd,xdf->sxnf", slotted, expert_up, preferred_element_type=jnp.float32
    )
    expert_hidden = (jax.nn.silu(expert_gate_pre) * expert_up_pre).astype(jnp.bfloat16)
    down_terms = jnp.einsum(
        "sxnf,xfd->sxnd", expert_hidden, expert_down, preferred_element_type=jnp.float32
    )
    rounded_terms = lax.optimization_barrier(down_terms.astype(jnp.bfloat16)).astype(jnp.float32)
    summed = sent_and_summed(rounded_terms.astype(jnp.bfloat16), "tp", 3)
    expert_rows = summed.astype(jnp.bfloat16).reshape(n_ep * experts_local, slot_count, slice_width)
    returned = lax.all_to_all(expert_rows, EP, split_axis=0, concat_axis=0, tiled=True)
    weighted = slot_match.astype(jnp.float32) * route_weights.reshape(-1)[:, None]
    combine = jnp.sum(weighted.reshape(seq_rows, top_count, experts_all * capacity), axis=1)
    routed = jnp.dot(
        combine,
        returned.reshape(experts_all * capacity, slice_width).astype(jnp.float32),
        precision=lax.Precision.HIGHEST,
    )
    branch_sum = routed + branch_mix[:, None] * shared_out.astype(jnp.float32)
    square_part = jnp.sum(branch_sum * branch_sum, axis=1)
    square_total = taken_together_2(square_part, "tp")
    norm_scale = lax.rsqrt(square_total / model_width + epsilon)
    resid_slice = lax.dynamic_slice_in_dim(
        resid, lax.axis_index("tp") * slice_width, slice_width, 1
    )
    layer_out = resid_slice.astype(jnp.float32) + branch_sum * norm_scale[
        :, None
    ] * gain_post.astype(jnp.float32)
    return (layer_out.astype(jnp.bfloat16), new_state)


def solution(mesh):
    torus = Mesh(mesh.devices.reshape(16, 4, 2, mesh.shape["tp"]), ("ep_0", "ep_1", "ep_2", "tp"))
    in_specs = (
        P(EP, None),
        P(EP, "tp", None, None),
        P(None, "tp"),
        P(None, "tp"),
        P(None, "tp"),
        P("tp", None),
        P("tp", None),
        P("tp", EP),
        P(),
        P(),
        P("tp"),
        P(),
        P(EP, "tp"),
        P(EP, "tp"),
        P("tp", EP),
        P(EP, None),
        P(EP, None),
        P(EP, None, "tp"),
        P(EP, None, "tp"),
        P(EP, "tp", None),
    )
    out_specs = (P(EP, "tp"), P(EP, "tp", None, None))
    return jax.shard_map(
        shards, mesh=torus, in_specs=in_specs, out_specs=out_specs, check_vma=False
    )
```

profile of v0, /device:TPU:32, one launch (start us, length us, event | category | flops | bytes accessed | tf_op | source)
XLA Modules:
  0.0 289.3 jit_solution(13542164941750039216)
XLA Ops:
  7.2 11.4 %all-gather = bf16[512,16]{0,1:T(8,128)(2,1)S(1)} all-gather(bf16[128,16]{0,1:T(8,128)(2,1)} %param.27), channel_id=2, replica_groups=mesh['ep_0'=16,'ep_1'=4,'ep_2'=2,'tp'=4] {'ep_1'}, dimensions={0}, use_global_device_ids=true | all-gather | bytes 20480 | tf_op jit(solution)/shard_map/all_gather | solution.py:22
  18.6 34.7 %all-gather.1 = bf16[64,128,16]{1,2,0:T(8,128)(2,1)S(1)} all-gather(bf16[4,128,16]{1,2,0:T(8,128)(2,1)S(1)} %copy_bitcast_fusion.1), channel_id=3, replica_groups=mesh['ep_0'=16,'ep_1'=4,'ep_2'=2,'tp'=4] {'ep_0'}, dimensions={0}, use_global_device_ids=true | all-gather | bytes 278528 | tf_op jit(solution)/shard_map/all_gather | solution.py:22
  53.3 2.3 all-gather.2
  57.0 1.0 multiply_add_fusion
  58.1 1.4 fusion.1
  60.0 0.8 broadcast_in_dim.6
  60.8 4.5 %all-to-all-start = ((bf16[4,24,2048]{2,1,0:T(8,128)(2,1)}), bf16[4,24,2048]{2,1,0:T(8,128)(2,1)S(1)}, u32[]{:S(2)}, u32[]{:S(2)}) async-start(bf16[4,24,2048]{2,1,0:T(8,128)(2,1)} %broadcast_in_dim.6), calls=%async_computation | async-start | bytes 786432 | tf_op jit(solution)/shard_map/all_to_all | solution.py:35
  66.0 7.6 %all-to-all-done = bf16[4,24,2048]{2,1,0:T(8,128)(2,1)S(1)} async-done(((bf16[4,24,2048]{2,1,0:T(8,128)(2,1)}), bf16[4,24,2048]{2,1,0:T(8,128)(2,1)S(1)}, u32[]{:S(2)}, u32[]{:S(2)}) %all-to-all-start) | async-done | bytes 393248 | tf_op jit(solution)/shard_map/all_to_all | solution.py:35
  74.3 0.6 convolution_convert_fusion.1
  74.9 1.5 reshape.192
  76.4 12.0 %all-to-all-start.1 = ((bf16[128,2,2048]{2,1,0:T(2,128)(2,1)}), bf16[128,2,2048]{2,1,0:T(2,128)(2,1)S(1)}, u32[]{:S(2)}, u32[]{:S(2)}) async-start(bf16[128,2,2048]{2,1,0:T(2,128)(2,1)} %reshape.192), calls=%async_computation.1 | async-start | bytes 2097152 | tf_op jit(solution)/shard_map/all_to_all | solution.py:159
  88.5 0.6 pad_maximum_fusion
  89.2 11.0 %all-gather.3 = bf16[512,16]{0,1:T(8,128)(2,1)S(1)} all-gather(bf16[128,16]{0,1:T(8,128)(2,1)S(1)} %copy-done.11), channel_id=5, replica_groups=mesh['ep_0'=16,'ep_1'=4,'ep_2'=2,'tp'=4] {'ep_1'}, dimensions={0}, use_global_device_ids=true | all-gather | bytes 20480 | tf_op jit(solution)/shard_map/all_gather | solution.py:22
  100.2 43.9 %all-to-all-done.1 = bf16[128,2,2048]{2,1,0:T(2,128)(2,1)S(1)} async-done(((bf16[128,2,2048]{2,1,0:T(2,128)(2,1)}), bf16[128,2,2048]{2,1,0:T(2,128)(2,1)S(1)}, u32[]{:S(2)}, u32[]{:S(2)}) %all-to-all-start.1) | async-done | bytes 1048608 | tf_op jit(solution)/shard_map/all_to_all | solution.py:159
  144.0 0.7 convolution_bitcast_fusion.1
  144.8 1.1 fusion
  145.9 1.1 copy.148
  147.0 3.5 %all-to-all-start.2 = ((bf16[4,128,1,2,512]{4,1,3,2,0:T(8,128)(2,1)}), bf16[4,128,1,2,512]{4,1,3,2,0:T(8,128)(2,1)S(1)}, u32[]{:S(2)}, u32[]{:S(2)}) async-start(bf16[4,128,1,2,512]{4,1,3,2,0:T(8,128)(2,1)} %bitcast.133), calls=%async_computation.2 | async-start | bytes 2097152 | tf_op jit(solution)/shard_map/all_to_all | solution.py:60
  150.5 28.1 %all-gather.4 = bf16[64,128,16]{1,2,0:T(8,128)(2,1)S(1)} all-gather(bf16[4,128,16]{1,2,0:T(8,128)(2,1)S(1)} %copy_bitcast_fusion), channel_id=6, replica_groups=mesh['ep_0'=16,'ep_1'=4,'ep_2'=2,'tp'=4] {'ep_0'}, dimensions={0}, use_global_device_ids=true | all-gather | bytes 278528 | tf_op jit(solution)/shard_map/all_gather | solution.py:22
  178.7 2.2 all-gather.5
  180.9 44.4 %all-gather.8.cloned.1.call-done = bf16[2048,256]{1,0:T(8,128)(2,1)} async-done(((bf16[16,256]{1,0:T(8,128)(2,1)}), bf16[2048,256]{1,0:T(8,128)(2,1)}) %all-gather.8.cloned.1.call-update) | async-done | bytes 1048592 | tf_op jit(solution)/shard_map/all_gather | solution.py:50
  225.3 1.2 fusion.17
  226.5 1.5 convolution_convert_fusion.2
  228.1 0.7 copy.149
  228.8 4.3 %all-to-all-start.4 = ((bf16[4,24,512]{2,1,0:T(8,128)(2,1)}), bf16[4,24,512]{2,1,0:T(8,128)(2,1)S(1)}, u32[]{:S(2)}, u32[]{:S(2)}) async-start(bf16[4,24,512]{2,1,0:T(8,128)(2,1)} %bitcast.128), calls=%async_computation.4 | async-start | bytes 196608 | tf_op jit(solution)/shard_map/all_to_all | solution.py:60
  233.3 1.0 copy.124
  234.3 4.6 %all-to-all-done.4 = bf16[4,24,512]{2,1,0:T(8,128)(2,1)S(1)} async-done(((bf16[4,24,512]{2,1,0:T(8,128)(2,1)}), bf16[4,24,512]{2,1,0:T(8,128)(2,1)S(1)}, u32[]{:S(2)}, u32[]{:S(2)}) %all-to-all-start.4) | async-done | bytes 98336 | tf_op jit(solution)/shard_map/all_to_all | solution.py:60
  238.8 11.0 %all-to-all-start.3 = ((bf16[128,2,512]{2,1,0:T(2,128)(2,1)}), bf16[128,2,512]{2,1,0:T(2,128)(2,1)S(1)}, u32[]{:S(2)}, u32[]{:S(2)}) async-start(bf16[128,2,512]{2,1,0:T(2,128)(2,1)} %copy.124), calls=%async_computation.3 | async-start | bytes 524288 | tf_op jit(solution)/shard_map/all_to_all | solution.py:175
  250.3 22.0 %all-to-all-done.3 = bf16[128,2,512]{2,1,0:T(2,128)(2,1)S(1)} async-done(((bf16[128,2,512]{2,1,0:T(2,128)(2,1)}), bf16[128,2,512]{2,1,0:T(2,128)(2,1)S(1)}, u32[]{:S(2)}, u32[]{:S(2)}) %all-to-all-start.3) | async-done | bytes 262176 | tf_op jit(solution)/shard_map/all_to_all | solution.py:175
  273.3 3.2 %all-to-all-start.5 = ((f32[4,1,24]{2,1,0:T(1,128)}), f32[4,1,24]{2,1,0:T(1,128)S(1)}, u32[]{:S(2)}, u32[]{:S(2)}) async-start(f32[4,1,24]{2,1,0:T(1,128)} %broadcast_in_dim.8), calls=%async_computation.5 | async-start | bytes 4096 | tf_op jit(solution)/shard_map/all_to_all | solution.py:35
  276.6 5.2 %all-to-all-done.5 = f32[4,1,24]{2,1,0:T(1,128)S(1)} async-done(((f32[4,1,24]{2,1,0:T(1,128)}), f32[4,1,24]{2,1,0:T(1,128)S(1)}, u32[]{:S(2)}, u32[]{:S(2)}) %all-to-all-start.5) | async-done | bytes 416 | tf_op jit(solution)/shard_map/all_to_all | solution.py:35
  281.8 0.7 add_convert_fusion
  (92 shorter events, 5.1 us)
Async XLA Ops:
  7.2 137.6 %copy-start = (bf16[1,128,2048]{2,1,0:T(8,128)(2,1)S(1)}, bf16[1,128,2048]{2,1,0:T(8,128)(2,1)}, u32[]{:S(2)}) copy-start(bf16[1,128,2048]{2,1,0:T(8,128)(2,1)} %param.39) | copy-start | bytes 1572868
  7.2 48.5 %copy-start.9 = (bf16[2048]{0:T(1024)(128)(2,1)S(1)}, bf16[2048]{0:T(1024)(128)(2,1)}, u32[]{:S(2)}) copy-start(bf16[2048]{0:T(1024)(128)(2,1)} %param.28) | copy-start | bytes 12292
  7.2 48.5 %copy-start.2 = (bf16[24,2048]{1,0:T(8,128)(2,1)S(1)}, bf16[24,2048]{1,0:T(8,128)(2,1)}, u32[]{:S(2)}) copy-start(bf16[24,2048]{1,0:T(8,128)(2,1)} %param.20) | copy-start | bytes 294916
  7.2 48.6 %copy-start.5 = (bf16[2048,128]{1,0:T(8,128)(2,1)S(1)}, bf16[2048,128]{1,0:T(8,128)(2,1)}, u32[]{:S(2)}) copy-start(bf16[2048,128]{1,0:T(8,128)(2,1)} %param.22) | copy-start | bytes 1572868
  7.2 48.9 %copy-start.6 = (bf16[2048,128]{1,0:T(8,128)(2,1)S(1)}, bf16[2048,128]{1,0:T(8,128)(2,1)}, u32[]{:S(2)}) copy-start(bf16[2048,128]{1,0:T(8,128)(2,1)} %param.24) | copy-start | bytes 1572868
  53.3 3.1 %copy-start.17 = (f32[1,128]{1,0:T(1,128)S(1)}, f32[1,128]{1,0:T(1,128)}, u32[]{:S(2)}) copy-start(f32[1,128]{1,0:T(1,128)} %param.25) | copy-start | bytes 1540
  53.3 3.1 %copy-start.19 = (bf16[1,128]{1,0:T(2,128)(2,1)S(1)}, bf16[1,128]{1,0:T(2,128)(2,1)}, u32[]{:S(2)}) copy-start(bf16[1,128]{1,0:T(2,128)(2,1)} %param.26) | copy-start | bytes 772
  53.3 3.1 %copy-start.7 = (bf16[2048,128]{1,0:T(8,128)(2,1)S(1)}, bf16[2048,128]{1,0:T(8,128)(2,1)}, u32[]{:S(2)}) copy-start(bf16[2048,128]{1,0:T(8,128)(2,1)} %param.23) | copy-start | bytes 1572868
  55.6 1.4 copy-start.3
  58.0 2.8 copy-start.1
  58.0 7.2 %copy-start.10 = (bf16[2048]{0:T(1024)(128)(2,1)S(1)}, bf16[2048]{0:T(1024)(128)(2,1)}, u32[]{:S(2)}) copy-start(bf16[2048]{0:T(1024)(128)(2,1)} %param.29) | copy-start | bytes 12292
  58.0 7.2 %copy-start.8 = (s32[24,6]{0,1:T(8,128)S(1)}, s32[24,6]{0,1:T(8,128)}, u32[]{:S(2)}) copy-start(s32[24,6]{0,1:T(8,128)} %param.35) | copy-start | bytes 1732
  60.8 12.8 %all-to-all-start = ((bf16[4,24,2048]{2,1,0:T(8,128)(2,1)}), bf16[4,24,2048]{2,1,0:T(8,128)(2,1)S(1)}, u32[]{:S(2)}, u32[]{:S(2)}) async-start(bf16[4,24,2048]{2,1,0:T(8,128)(2,1)} %broadcast_in_dim.6), calls=%async_computation | async-start | bytes 786432 | tf_op jit(solution)/shard_map/all_to_all | solution.py:35
  76.4 12.1 %copy-start.13 = (bf16[16,128]{1,0:T(8,128)(2,1)S(1)}, bf16[16,128]{1,0:T(8,128)(2,1)}, u32[]{:S(2)}) copy-start(bf16[16,128]{1,0:T(8,128)(2,1)} %param.33) | copy-start | bytes 12292
  76.4 12.1 %copy-start.14 = (bf16[16,128]{1,0:T(8,128)(2,1)S(1)}, bf16[16,128]{1,0:T(8,128)(2,1)}, u32[]{:S(2)}) copy-start(bf16[16,128]{1,0:T(8,128)(2,1)} %param.32) | copy-start | bytes 12292
  76.4 12.7 %copy-start.11 = (bf16[128,16]{0,1:T(8,128)(2,1)S(1)}, bf16[128,16]{0,1:T(8,128)(2,1)}, u32[]{:S(2)}) copy-start(bf16[128,16]{0,1:T(8,128)(2,1)} %param.34) | copy-start | bytes 12292
  76.4 67.6 %copy-start.18 = (bf16[1,2048,128]{2,1,0:T(8,128)(2,1)S(1)}, bf16[1,2048,128]{2,1,0:T(8,128)(2,1)}, u32[]{:S(2)}) copy-start(bf16[1,2048,128]{2,1,0:T(8,128)(2,1)} %param.37) | copy-start | bytes 1572868
  76.4 68.4 %copy-start.4 = (bf16[1,2048,128]{2,1,0:T(8,128)(2,1)S(1)}, bf16[1,2048,128]{2,1,0:T(8,128)(2,1)}, u32[]{:S(2)}) copy-start(bf16[1,2048,128]{2,1,0:T(8,128)(2,1)} %param.38) | copy-start | bytes 1572868
  76.4 67.6 %all-to-all-start.1 = ((bf16[128,2,2048]{2,1,0:T(2,128)(2,1)}), bf16[128,2,2048]{2,1,0:T(2,128)(2,1)S(1)}, u32[]{:S(2)}, u32[]{:S(2)}) async-start(bf16[128,2,2048]{2,1,0:T(2,128)(2,1)} %reshape.192), calls=%async_computation.1 | async-start | bytes 2097152 | tf_op jit(solution)/shard_map/all_to_all | solution.py:159
  88.4 136.9 %all-gather.8.cloned.1.call-start = ((), (), s32[]{:S(2)}) async-start(), calls=%async_computation.6 | async-start | bytes 1056768 | tf_op jit(solution)/shard_map/all_gather | solution.py:50
  147.0 81.8 %all-to-all-start.2 = ((bf16[4,128,1,2,512]{4,1,3,2,0:T(8,128)(2,1)}), bf16[4,128,1,2,512]{4,1,3,2,0:T(8,128)(2,1)S(1)}, u32[]{:S(2)}, u32[]{:S(2)}) async-start(bf16[4,128,1,2,512]{4,1,3,2,0:T(8,128)(2,1)} %bitcast.133), calls=%async_computation.2 | async-start | bytes 2097152 | tf_op jit(solution)/shard_map/all_to_all | solution.py:60
  228.1 21.8 %copy-start.12 = (bf16[2048]{0:T(1024)(128)(2,1)S(1)}, bf16[2048]{0:T(1024)(128)(2,1)}, u32[]{:S(2)}) copy-start(bf16[2048]{0:T(1024)(128)(2,1)} %param.31) | copy-start | bytes 12292
  228.1 21.9 %copy-start.16 = (bf16[512]{0:T(512)(128)(2,1)S(1)}, bf16[512]{0:T(512)(128)(2,1)}, u32[]{:S(2)}) copy-start(bf16[512]{0:T(512)(128)(2,1)} %param.30) | copy-start | bytes 3076
  228.1 21.9 %copy-start.15 = (f32[24,6]{0,1:T(8,128)S(1)}, f32[24,6]{0,1:T(8,128)}, u32[]{:S(2)}) copy-start(f32[24,6]{0,1:T(8,128)} %param.36) | copy-start | bytes 1732
  228.8 10.1 %all-to-all-start.4 = ((bf16[4,24,512]{2,1,0:T(8,128)(2,1)}), bf16[4,24,512]{2,1,0:T(8,128)(2,1)S(1)}, u32[]{:S(2)}, u32[]{:S(2)}) async-start(bf16[4,24,512]{2,1,0:T(8,128)(2,1)} %bitcast.128), calls=%async_computation.4 | async-start | bytes 196608 | tf_op jit(solution)/shard_map/all_to_all | solution.py:60
  238.8 33.5 %all-to-all-start.3 = ((bf16[128,2,512]{2,1,0:T(2,128)(2,1)}), bf16[128,2,512]{2,1,0:T(2,128)(2,1)S(1)}, u32[]{:S(2)}, u32[]{:S(2)}) async-start(bf16[128,2,512]{2,1,0:T(2,128)(2,1)} %copy.124), calls=%async_computation.3 | async-start | bytes 524288 | tf_op jit(solution)/shard_map/all_to_all | solution.py:175
  273.3 8.4 %all-to-all-start.5 = ((f32[4,1,24]{2,1,0:T(1,128)}), f32[4,1,24]{2,1,0:T(1,128)S(1)}, u32[]{:S(2)}, u32[]{:S(2)}) async-start(f32[4,1,24]{2,1,0:T(1,128)} %broadcast_in_dim.8), calls=%async_computation.5 | async-start | bytes 4096 | tf_op jit(solution)/shard_map/all_to_all | solution.py:35
Sparse Core Ops, SparseCore 0:
  92.8 132.4 all-gather.7
where the time goes:
time: 290 us; the launch traced here: 289 us
  waiting for transfers between devices  128 us (44%)
  blocking collectives  89.7 us (31%)
  starting transfers between devices  38.5 us (13%)
  between operations  14.5 us (5%)
  matrix products  8.25 us (3%)
  local copies, waits for them, and re-layouts  6.94 us (2%)
  other arithmetic  3.8 us (1%)
    all_gather x6, blocking collectives, gather_in_order(): parts = lax.all_gather(parts, axes[k])  89.7 us
    all_gather x1, waiting for transfers between devices, sent_together(): lax.all_gather(both, axis, axis=dim, tiled=True)  44.4 us
    all_to_all x1, waiting for transfers between devices, shards(): lax.all_to_all(send_rows, EP, split_axis=0, concat_axis=0, tiled=True)  43.9 us
    all_to_all x1, waiting for transfers between devices, shards(): lax.all_to_all(expert_rows, EP, split_axis=0, concat_axis=0, tiled=True)  22 us
    all_to_all x2, waiting for transfers between devices, sent_to_all(): lax.all_to_all(jnp.broadcast_to(value[None], (devices, *value.shape)), ax...  12.8 us
    all_to_all x1, starting transfers between devices, shards(): lax.all_to_all(send_rows, EP, split_axis=0, concat_axis=0, tiled=True)  12 us
    all_to_all x1, starting transfers between devices, shards(): lax.all_to_all(expert_rows, EP, split_axis=0, concat_axis=0, tiled=True)  11 us
    all_to_all x2, starting transfers between devices, sent_and_summed(): lax.all_to_all(in_blocks(value, dim, devices), axis, 0, 0, tiled=True)  7.8 us
  transfers between devices with their start and end apart: 7, of which 6 were waited for; matrix products, arithmetic and copies ran while one was open for 3% of the time, Pallas kernels for 0%

commit v1 on v0

v1 whole, which is shorter than its diff:
```python
import jax
import jax.numpy as jnp
from jax import lax
from jax.experimental import pallas as pl
from jax.experimental.pallas import tpu as pltpu
from jax.sharding import Mesh
from jax.sharding import PartitionSpec as P

EP = ("ep_0", "ep_1", "ep_2")
epsilon = 1e-06
BF = jnp.bfloat16
F32 = jnp.float32
NT = (((1,), (1,)), ((), ()))


def exchanged(value, axes, name):
    with jax.named_scope(name):
        return lax.all_to_all(value, axes, 0, 0, tiled=True)


def to_all(value, axes, name):
    devices = lax.axis_size(axes)
    return exchanged(jnp.broadcast_to(value[None], (devices, *value.shape)), axes, name)


def rmsnorm(values_in, gain):
    scale = lax.rsqrt(jnp.mean(values_in * values_in, axis=-1, keepdims=True) + epsilon)
    return values_in * scale * gain.astype(F32)


def expert_body(
    x, gain, mix_w, gate_w, up_w, down_w, sgate_w, sup_w, sdown_w, out, mix, hn
):
    n_tp, total, slice_width = x.shape
    width = n_tp * slice_width
    own = mix.shape[0]
    rows = total - own
    squares = jnp.zeros((total, 1), F32)
    for j in range(n_tp):
        wide = x[j].astype(F32)
        squares = squares + jnp.sum(wide * wide, axis=1, keepdims=True)
    scale = lax.rsqrt(squares / width + epsilon)
    logits = jnp.zeros((own, 1), F32)
    for j in range(n_tp):
        cols = pl.ds(j * slice_width, slice_width)
        part = (x[j].astype(F32) * scale * gain[:, cols].astype(F32)).astype(BF)
        hn[:, cols] = part
        logits = logits + jnp.sum(
            part[rows:].astype(F32) * mix_w[:, cols].astype(F32), axis=1, keepdims=True
        )
    mix[...] = jnp.broadcast_to(jax.nn.sigmoid(logits), mix.shape)
    routed = hn[:rows, :]
    gate_pre = jnp.dot(routed, gate_w[...], preferred_element_type=F32)
    up_pre = jnp.dot(routed, up_w[...], preferred_element_type=F32)
    hidden = (gate_pre * jax.nn.sigmoid(gate_pre) * up_pre).astype(BF)
    mine = hn[rows:, :]
    gate_pre = jnp.dot(mine, sgate_w[...], preferred_element_type=F32)
    up_pre = jnp.dot(mine, sup_w[...], preferred_element_type=F32)
    shared_hidden = (gate_pre * jax.nn.sigmoid(gate_pre) * up_pre).astype(BF)
    for j in range(n_tp):
        cols = pl.ds(j * slice_width, slice_width)
        out[j, :rows, :] = jnp.dot(hidden, down_w[:, cols], preferred_element_type=F32).astype(BF)
        out[j, rows:, :] = lax.dot_general(
            shared_hidden, sdown_w[cols, :], NT, preferred_element_type=F32
        ).astype(BF)


def expert_kernel(own, x, *rest):
    n_tp, total, slice_width = x.shape
    vmem = pl.BlockSpec(memory_space=pltpu.VMEM)
    return pl.pallas_call(
        expert_body,
        out_shape=(
            jax.ShapeDtypeStruct(x.shape, BF),
            jax.ShapeDtypeStruct((own, 128), F32),
        ),
        in_specs=[vmem] * 9,
        out_specs=(vmem, vmem),
        scratch_shapes=[pltpu.VMEM((total, n_tp * slice_width), BF)],
        compiler_params=pltpu.CompilerParams(vmem_limit_bytes=32 * 1024 * 1024),
        name="expert",
    )(x, *rest)


def shards(
    tokens,
    carried_state,
    w_query,
    w_forget,
    w_value,
    forget_floor,
    head_gain,
    w_out,
    gain_mix,
    gain_ffn,
    gain_post,
    w_branch_gate,
    shared_gate,
    shared_up,
    shared_down,
    routes,
    route_weights,
    expert_gate,
    expert_up,
    expert_down,
):
    seq_rows, model_width = tokens.shape
    head_dim = carried_state.shape[2]
    n_ep = lax.axis_size(EP)
    n_tp = lax.axis_size("tp")
    slice_width = model_width // n_tp
    blocks = slice_width // 128
    here = lax.axis_index("tp")
    parts = to_all(jnp.stack([w_out.T, shared_gate, shared_up, shared_down.T]), "ep_0", "wz")
    wt = to_all(parts[:, 0], "ep_1", "wx")
    wt = to_all(wt, "ep_2", "wc")
    wt = wt.transpose(2, 1, 0, 3, 4).reshape(model_width, head_dim)
    expert_ids = lax.broadcasted_iota(jnp.int32, (1, 1, n_ep), 2)
    hits = routes[:, :, None] == expert_ids
    named = jnp.any(hits, axis=1).astype(BF)
    tri = (
        lax.broadcasted_iota(jnp.int32, (seq_rows, seq_rows), 0)
        > lax.broadcasted_iota(jnp.int32, (seq_rows, seq_rows), 1)
    ).astype(BF)
    rank = jnp.dot(tri, named, preferred_element_type=F32)
    slots = [
        jnp.where((named > 0) & (rank == s), 1.0, 0.0).astype(BF) for s in range(2)
    ]
    slot = jnp.stack(slots, axis=2)
    weights = jnp.sum(jnp.where(hits, route_weights[:, :, None], 0.0), axis=1)
    normed = rmsnorm(tokens.astype(F32), gain_mix).astype(BF)
    queries = jax.nn.silu(jnp.dot(normed, w_query, preferred_element_type=F32))
    forget_pre = jnp.dot(normed, w_forget, preferred_element_type=F32)
    values_in = jnp.dot(normed, w_value, preferred_element_type=F32)
    queries = queries.reshape(seq_rows, 1, head_dim)
    forget_pre = forget_pre.reshape(seq_rows, 1, head_dim)
    values_in = values_in.reshape(seq_rows, 1, head_dim)
    forget = forget_floor + (1.0 - forget_floor) * jax.nn.sigmoid(forget_pre)
    keys_in = (1.0 - forget_floor) * jax.nn.sigmoid(-forget_pre)
    new_state = forget[..., None] * carried_state + keys_in[..., None] * values_in[:, :, None, :]
    readout = jnp.einsum("bhd,bhdv->bhv", queries, new_state, precision=lax.Precision.HIGHEST)
    head_out = rmsnorm(readout, head_gain).astype(BF).reshape(seq_rows, head_dim)
    terms = lax.dot_general(head_out, wt, NT, preferred_element_type=F32).astype(BF)
    terms = terms.reshape(seq_rows, n_tp, slice_width).transpose(1, 0, 2)
    mixed = jnp.sum(exchanged(terms, "tp", "mix").astype(F32), axis=0).astype(BF)
    token_slice = lax.dynamic_slice_in_dim(tokens, here * slice_width, slice_width, 1)
    resid = (token_slice.astype(F32) + mixed.astype(F32)).astype(BF)
    sent = jnp.einsum("bes,bd->esd", slot, resid, preferred_element_type=F32).astype(BF)
    arrived = exchanged(sent.reshape(n_ep, 2 * blocks, 128), EP, "disp")
    arrived = arrived.reshape(2 * n_ep, slice_width)
    with jax.named_scope("sx"):
        shared = lax.all_gather(parts[:, 1:], "ep_1")
    with jax.named_scope("sc"):
        other = lax.ppermute(shared, "ep_2", [(0, 1), (1, 0)])
        first = lax.axis_index("ep_2") == 0
        shared = jnp.stack([jnp.where(first, shared, other), jnp.where(first, other, shared)])
    shared = shared.transpose(3, 2, 1, 0, 4, 5).reshape(3, model_width, head_dim)
    x = to_all(jnp.concatenate([arrived, resid], axis=0), "tp", "rows")
    down_terms, mix = expert_kernel(
        seq_rows,
        x,
        gain_ffn[None],
        w_branch_gate[None],
        expert_gate[0],
        expert_up[0],
        expert_down[0],
        shared[0],
        shared[1],
        shared[2],
    )
    summed = jnp.sum(exchanged(down_terms, "tp", "rs").astype(F32), axis=0).astype(BF)
    returned = exchanged(summed[: 2 * n_ep].reshape(n_ep, 2 * blocks, 128), EP, "ret")
    shared_out = summed[2 * n_ep :]
    combine = weights[:, :, None] * slot.astype(F32)
    routed = jnp.dot(
        combine.reshape(seq_rows, 2 * n_ep),
        returned.reshape(2 * n_ep, slice_width).astype(F32),
        precision=lax.Precision.HIGHEST,
    )
    branch_sum = routed + mix[:, :1] * shared_out.astype(F32)
    square_part = jnp.sum(branch_sum * branch_sum, axis=1)
    square_total = jnp.sum(to_all(square_part, "tp", "sq"), axis=0)
    norm_scale = lax.rsqrt(square_total / model_width + epsilon)
    layer_out = resid.astype(F32) + branch_sum * norm_scale[:, None] * gain_post.astype(F32)
    return (layer_out.astype(BF), new_state)


def solution(mesh):
    torus = Mesh(mesh.devices.reshape(16, 4, 2, mesh.shape["tp"]), ("ep_0", "ep_1", "ep_2", "tp"))
    in_specs = (
        P(EP, None),
        P(EP, "tp", None, None),
        P(None, "tp"),
        P(None, "tp"),
        P(None, "tp"),
        P("tp", None),
        P("tp", None),
        P("tp", EP),
        P(),
        P(),
        P("tp"),
        P(),
        P(EP, "tp"),
        P(EP, "tp"),
        P("tp", EP),
        P(EP, None),
        P(EP, None),
        P(EP, None, "tp"),
        P(EP, None, "tp"),
        P(EP, "tp", None),
    )
    out_specs = (P(EP, "tp"), P(EP, "tp", None, None))
    return jax.shard_map(
        shards, mesh=torus, in_specs=in_specs, out_specs=out_specs, check_vma=False
    )
```

time: 290 us -> 186 us (0.64)
  waiting for transfers between devices: 128 us -> 71.1 us
  blocking collectives: 89.7 us -> 37.1 us
  starting transfers between devices: 38.5 us -> 52.1 us
  between operations: 14.5 us -> 1.1 us
  matrix products: 8.25 us -> 4.39 us
  local copies, waits for them, and re-layouts: 6.94 us -> 10.3 us
  other arithmetic: 3.8 us -> 7.03 us
    all_gather x6 -> x1, blocking collectives: 89.7 us -> 14.6 us  [shards(): shared = lax.all_gather(parts[:, 1:], 'ep_1')]
    all_gather x1 -> x0, waiting for transfers between devices: 44.4 us -> none  [sent_together(): lax.all_gather(both, axis, axis=dim, tiled=True)]
    all_to_all x0 -> x2, blocking collectives: none -> 22.5 us  [exchanged(): return lax.all_to_all(value, axes, 0, 0, tiled=True)]
    all_to_all x6 -> x7, waiting for transfers between devices: 83.2 us -> 71.1 us  [exchanged(): return lax.all_to_all(value, axes, 0, 0, tiled=True)]
    all_to_all x6 -> x7, starting transfers between devices: 38.4 us -> 50.2 us  [exchanged(): return lax.all_to_all(value, axes, 0, 0, tiled=True)]
    dot_general x11 -> x7, matrix products: 6.84 us -> 2.97 us  [the longest x1 1.33 us: shards(): values_in = jnp.dot(normed, w_value, preferred_element_type=F32)]
  transfers between devices with their start and end apart: 7 -> 8, of which waited for: 6 -> 7; matrix products, arithmetic and copies ran while one was open for 3% -> 6% of each run, Pallas kernels for 0% -> 0%
where the time goes in v1:
time: 186 us; the launch traced here: 185 us
  waiting for transfers between devices  71.1 us (38%)
  starting transfers between devices  52.1 us (28%)
  blocking collectives  37.1 us (20%)
  local copies, waits for them, and re-layouts  10.3 us (6%)
  other arithmetic  7.03 us (4%)
  matrix products  4.39 us (2%)
    all_to_all x7, waiting for transfers between devices, exchanged(): return lax.all_to_all(value, axes, 0, 0, tiled=True)  71.1 us
    all_to_all x7, starting transfers between devices, exchanged(): return lax.all_to_all(value, axes, 0, 0, tiled=True)  50.2 us
    all_to_all x2, blocking collectives, exchanged(): return lax.all_to_all(value, axes, 0, 0, tiled=True)  22.5 us
    all_gather x1, blocking collectives, shards(): shared = lax.all_gather(parts[:, 1:], 'ep_1')  14.6 us
  transfers between devices with their start and end apart: 8, of which 7 were waited for; matrix products, arithmetic and copies ran while one was open for 6% of the time, Pallas kernels for 0%

profile of v1, /device:TPU:32, one launch (start us, length us, event | category | flops | bytes accessed | tf_op | source)
XLA Modules:
  0.0 184.6 jit_solution(11878658642901539831)
XLA Ops:
  0.7 0.8 pad_maximum_fusion.1
  1.5 0.7 broadcast_in_dim.34
  2.2 15.2 %all-to-all-start = ((bf16[16,4,16,128]{3,2,1,0:T(8,128)(2,1)}), bf16[16,4,16,128]{3,2,1,0:T(8,128)(2,1)S(1)}, u32[]{:S(2)}, u32[]{:S(2)}) async-start(bf16[16,4,16,128]{3,2,1,0:T(8,128)(2,1)} %broadcast_in_dim.34), calls=%async_computation | async-start | bytes 524288 | tf_op jit(solution)/shard_map/wz/all_to_all | solution.py:18
  18.1 1.0 fusion.2
  19.8 1.3 fusion.13
  21.5 2.2 %multiply_add_fusion = f32[24,1,128,128]{3,2,1,0:T(8,128)S(1)} fusion(f32[24,1,128,128]{3,2,1,0:T(8,128)} %param.21, f32[24,128]{1,0:T(8,128)S(1)} %fusion.13, f32[24,128]{1,0:T(8,128)S(1)} %get-tuple-element.14, f32[24,128]{1,0:T(8,128)S(1)} %get-tuple-element.13), kind=kLoop, calls=%fused_computation.4 | loop fusion | flops 1179648 | bytes 3182592 | tf_op jit(solution)/shard_map/add | solution.py:140
  24.0 1.4 fusion
  25.7 9.7 %all-to-all-done = bf16[16,4,16,128]{3,2,1,0:T(8,128)(2,1)S(1)} async-done(((bf16[16,4,16,128]{3,2,1,0:T(8,128)(2,1)}), bf16[16,4,16,128]{3,2,1,0:T(8,128)(2,1)S(1)}, u32[]{:S(2)}, u32[]{:S(2)}) %all-to-all-start) | async-done | bytes 262176 | tf_op jit(solution)/shard_map/wz/all_to_all | solution.py:18
  35.4 0.7 broadcast_in_dim.36
  36.1 4.3 %all-to-all-start.1 = ((bf16[4,16,16,128]{3,2,1,0:T(8,128)(2,1)}), bf16[4,16,16,128]{3,2,1,0:T(8,128)(2,1)S(1)}, u32[]{:S(2)}, u32[]{:S(2)}) async-start(bf16[4,16,16,128]{3,2,1,0:T(8,128)(2,1)} %broadcast_in_dim.36), calls=%async_computation.1 | async-start | bytes 524288 | tf_op jit(solution)/shard_map/wx/all_to_all | solution.py:18
  40.4 6.7 %all-to-all-done.1 = bf16[4,16,16,128]{3,2,1,0:T(8,128)(2,1)S(1)} async-done(((bf16[4,16,16,128]{3,2,1,0:T(8,128)(2,1)}), bf16[4,16,16,128]{3,2,1,0:T(8,128)(2,1)S(1)}, u32[]{:S(2)}, u32[]{:S(2)}) %all-to-all-start.1) | async-done | bytes 262176 | tf_op jit(solution)/shard_map/wx/all_to_all | solution.py:18
  47.2 4.2 %all_to_all.46 = bf16[2,4,16,16,128]{4,3,1,2,0:T(8,128)(2,1)S(1)} all-to-all(bf16[2,4,16,16,128]{4,3,1,2,0:T(8,128)(2,1)S(1)} %broadcast_in_dim.37), channel_id=1, replica_groups=mesh['ep_0'=16,'ep_1'=4,'ep_2'=2,'tp'=4] {'ep_2'}, dimensions={0} | all-to-all | bytes 1048576 | tf_op jit(solution)/shard_map/wc/all_to_all | solution.py:18
  52.5 4.5 %all-to-all-start.3 = ((bf16[4,24,512]{2,1,0:T(8,128)(2,1)}), bf16[4,24,512]{2,1,0:T(8,128)(2,1)S(1)}, u32[]{:S(2)}, u32[]{:S(2)}) async-start(bf16[4,24,512]{2,1,0:T(8,128)(2,1)} %bitcast.64), calls=%async_computation.3 | async-start | bytes 196608 | tf_op jit(solution)/shard_map/mix/all_to_all | solution.py:18
  57.1 5.7 %all-to-all-done.3 = bf16[4,24,512]{2,1,0:T(8,128)(2,1)S(1)} async-done(((bf16[4,24,512]{2,1,0:T(8,128)(2,1)}), bf16[4,24,512]{2,1,0:T(8,128)(2,1)S(1)}, u32[]{:S(2)}, u32[]{:S(2)}) %all-to-all-start.3) | async-done | bytes 98336 | tf_op jit(solution)/shard_map/mix/all_to_all | solution.py:18
  63.2 0.9 copy.65
  64.1 8.2 %all-to-all-start.4 = ((bf16[128,8,128]{2,1,0:T(8,128)(2,1)}), bf16[128,8,128]{2,1,0:T(8,128)(2,1)S(1)}, u32[]{:S(2)}, u32[]{:S(2)}) async-start(bf16[128,8,128]{2,1,0:T(8,128)(2,1)} %copy.65), calls=%async_computation.4 | async-start | bytes 524288 | tf_op jit(solution)/shard_map/disp/all_to_all | solution.py:18
  72.3 14.6 %all-gather = bf16[64,3,16,128]{3,2,1,0:T(8,128)(2,1)S(1)} all-gather(bf16[16,3,16,128]{3,2,1,0:T(8,128)(2,1)S(1)} %slice.36), channel_id=2, replica_groups=mesh['ep_0'=16,'ep_1'=4,'ep_2'=2,'tp'=4] {'ep_1'}, dimensions={0}, use_global_device_ids=true | all-gather | bytes 983040 | tf_op jit(solution)/shard_map/sx/all_gather | solution.py:152
  86.9 1.9 %collective-permute-start = (bf16[4,16,3,16,128]{4,3,2,1,0:T(8,128)(2,1)S(1)}, bf16[4,16,3,16,128]{4,3,2,1,0:T(8,128)(2,1)S(1)}, u32[]{:S(2)}, u32[]{:S(2)}) collective-permute-start(bf16[4,16,3,16,128]{4,3,2,1,0:T(8,128)(2,1)S(1)} %bitcast.71), channel_id=1, source_target_pairs={{0,4},{4,0},{1,5},{5,1},{2,6},{6,2},{3,7},{7,3},{8,12},{12,8},{9,1... | collective-permute-start | bytes 2359304 | tf_op jit(solution)/shard_map/sc/ppermute | solution.py:154
  88.8 6.0 %all-to-all-done.4 = bf16[128,8,128]{2,1,0:T(8,128)(2,1)S(1)} async-done(((bf16[128,8,128]{2,1,0:T(8,128)(2,1)}), bf16[128,8,128]{2,1,0:T(8,128)(2,1)S(1)}, u32[]{:S(2)}, u32[]{:S(2)}) %all-to-all-start.4) | async-done | bytes 262176 | tf_op jit(solution)/shard_map/disp/all_to_all | solution.py:18
  95.0 1.1 broadcast_in_dim.40
  96.1 3.5 %all-to-all-start.5 = ((bf16[4,280,512]{2,1,0:T(8,128)(2,1)}), bf16[4,280,512]{2,1,0:T(8,128)(2,1)S(1)}, u32[]{:S(2)}, u32[]{:S(2)}) async-start(bf16[4,280,512]{2,1,0:T(8,128)(2,1)} %broadcast_in_dim.40), calls=%async_computation.5 | async-start | bytes 2293760 | tf_op jit(solution)/shard_map/rows/all_to_all | solution.py:18
  100.6 15.8 %all-to-all-done.5.x = bf16[4,280,512]{2,1,0:T(8,128)(2,1)S(1)} async-done(((bf16[4,280,512]{2,1,0:T(8,128)(2,1)}), bf16[4,280,512]{2,1,0:T(8,128)(2,1)S(1)}, u32[]{:S(2)}, u32[]{:S(2)}) %all-to-all-start.5) | async-done | bytes 1146912 | tf_op jit(solution)/shard_map/rows/all_to_all | solution.py:18
  116.4 1.0 copy-done.1
  117.4 1.0 copy-done.2
  118.5 1.0 copy-done.3
  119.5 1.5 expert.1
  121.0 18.3 %all_to_all.47 = bf16[4,280,512]{2,1,0:T(8,128)(2,1)S(1)} all-to-all(bf16[4,280,512]{2,1,0:T(8,128)(2,1)S(1)} %get-tuple-element.4), channel_id=1, replica_groups=mesh['ep_0'=16,'ep_1'=4,'ep_2'=2,'tp'=4] {'tp'}, dimensions={0} | all-to-all | bytes 2293760 | tf_op jit(solution)/shard_map/rs/all_to_all | solution.py:18
  139.7 0.9 reshape.137
  140.5 11.3 %all-to-all-start.7 = ((bf16[128,8,128]{2,1,0:T(8,128)(2,1)}), bf16[128,8,128]{2,1,0:T(8,128)(2,1)S(1)}, u32[]{:S(2)}, u32[]{:S(2)}) async-start(bf16[128,8,128]{2,1,0:T(8,128)(2,1)} %reshape.137), calls=%async_computation.7 | async-start | bytes 524288 | tf_op jit(solution)/shard_map/ret/all_to_all | solution.py:18
  152.2 22.1 %all-to-all-done.7 = bf16[128,8,128]{2,1,0:T(8,128)(2,1)S(1)} async-done(((bf16[128,8,128]{2,1,0:T(8,128)(2,1)}), bf16[128,8,128]{2,1,0:T(8,128)(2,1)S(1)}, u32[]{:S(2)}, u32[]{:S(2)}) %all-to-all-start.7) | async-done | bytes 262176 | tf_op jit(solution)/shard_map/ret/all_to_all | solution.py:18
  175.4 3.2 %all-to-all-start.8 = ((f32[4,1,24]{2,1,0:T(1,128)}), f32[4,1,24]{2,1,0:T(1,128)S(1)}, u32[]{:S(2)}, u32[]{:S(2)}) async-start(f32[4,1,24]{2,1,0:T(1,128)} %broadcast_in_dim.43), calls=%async_computation.8 | async-start | bytes 4096 | tf_op jit(solution)/shard_map/sq/all_to_all | solution.py:18
  178.7 5.2 %all-to-all-done.8 = f32[4,1,24]{2,1,0:T(1,128)S(1)} async-done(((f32[4,1,24]{2,1,0:T(1,128)}), f32[4,1,24]{2,1,0:T(1,128)S(1)}, u32[]{:S(2)}, u32[]{:S(2)}) %all-to-all-start.8) | async-done | bytes 416 | tf_op jit(solution)/shard_map/sq/all_to_all | solution.py:18
  (70 shorter events, 7.5 us)
Async XLA Ops:
  0.6 20.5 %copy-start = (bf16[2048,128]{1,0:T(8,128)(2,1)S(1)}, bf16[2048,128]{1,0:T(8,128)(2,1)}, u32[]{:S(2)}) copy-start(bf16[2048,128]{1,0:T(8,128)(2,1)} %param.23) | copy-start | bytes 1572868
  0.6 20.5 %copy-start.12 = (f32[1,128]{1,0:T(1,128)S(1)}, f32[1,128]{1,0:T(1,128)}, u32[]{:S(2)}) copy-start(f32[1,128]{1,0:T(1,128)} %param.25) | copy-start | bytes 1540
  0.7 20.5 %copy-start.5 = (bf16[24,2048]{1,0:T(8,128)(2,1)S(1)}, bf16[24,2048]{1,0:T(8,128)(2,1)}, u32[]{:S(2)}) copy-start(bf16[24,2048]{1,0:T(8,128)(2,1)} %param.20) | copy-start | bytes 294916
  2.2 33.1 %all-to-all-start = ((bf16[16,4,16,128]{3,2,1,0:T(8,128)(2,1)}), bf16[16,4,16,128]{3,2,1,0:T(8,128)(2,1)S(1)}, u32[]{:S(2)}, u32[]{:S(2)}) async-start(bf16[16,4,16,128]{3,2,1,0:T(8,128)(2,1)} %broadcast_in_dim.34), calls=%async_computation | async-start | bytes 524288 | tf_op jit(solution)/shard_map/wz/all_to_all | solution.py:18
  21.5 2.3 %copy-start.6 = (bf16[2048,128]{1,0:T(8,128)(2,1)S(1)}, bf16[2048,128]{1,0:T(8,128)(2,1)}, u32[]{:S(2)}) copy-start(bf16[2048,128]{1,0:T(8,128)(2,1)} %param.22) | copy-start | bytes 1572868
  23.7 12.4 %copy-start.4 = (f32[24,1,128,128]{3,2,1,0:T(8,128)}, f32[24,1,128,128]{3,2,1,0:T(8,128)S(1)}, u32[]{:S(2)}) copy-start(f32[24,1,128,128]{3,2,1,0:T(8,128)S(1)} %multiply_add_fusion) | copy-start | bytes 4718596
  23.7 1.8 copy-start.7
  23.7 1.9 %copy-start.13 = (bf16[1,128]{1,0:T(2,128)(2,1)S(1)}, bf16[1,128]{1,0:T(2,128)(2,1)}, u32[]{:S(2)}) copy-start(bf16[1,128]{1,0:T(2,128)(2,1)} %param.26) | copy-start | bytes 772
  36.1 11.0 %all-to-all-start.1 = ((bf16[4,16,16,128]{3,2,1,0:T(8,128)(2,1)}), bf16[4,16,16,128]{3,2,1,0:T(8,128)(2,1)S(1)}, u32[]{:S(2)}, u32[]{:S(2)}) async-start(bf16[4,16,16,128]{3,2,1,0:T(8,128)(2,1)} %broadcast_in_dim.36), calls=%async_computation.1 | async-start | bytes 524288 | tf_op jit(solution)/shard_map/wx/all_to_all | solution.py:18
  52.5 10.3 %all-to-all-start.3 = ((bf16[4,24,512]{2,1,0:T(8,128)(2,1)}), bf16[4,24,512]{2,1,0:T(8,128)(2,1)S(1)}, u32[]{:S(2)}, u32[]{:S(2)}) async-start(bf16[4,24,512]{2,1,0:T(8,128)(2,1)} %bitcast.64), calls=%async_computation.3 | async-start | bytes 196608 | tf_op jit(solution)/shard_map/mix/all_to_all | solution.py:18
  64.1 30.7 %all-to-all-start.4 = ((bf16[128,8,128]{2,1,0:T(8,128)(2,1)}), bf16[128,8,128]{2,1,0:T(8,128)(2,1)S(1)}, u32[]{:S(2)}, u32[]{:S(2)}) async-start(bf16[128,8,128]{2,1,0:T(8,128)(2,1)} %copy.65), calls=%async_computation.4 | async-start | bytes 524288 | tf_op jit(solution)/shard_map/disp/all_to_all | solution.py:18
  86.9 12.8 %collective-permute-start = (bf16[4,16,3,16,128]{4,3,2,1,0:T(8,128)(2,1)S(1)}, bf16[4,16,3,16,128]{4,3,2,1,0:T(8,128)(2,1)S(1)}, u32[]{:S(2)}, u32[]{:S(2)}) collective-permute-start(bf16[4,16,3,16,128]{4,3,2,1,0:T(8,128)(2,1)S(1)} %bitcast.71), channel_id=1, source_target_pairs={{0,4},{4,0},{1,5},{5,1},{2,6},{6,2},{3,7},{7,3},{8,12},{12,8},{9,1... | collective-permute-start | bytes 2359304 | tf_op jit(solution)/shard_map/sc/ppermute | solution.py:154
  95.0 4.7 %copy-start.8 = (bf16[2048]{0:T(1024)(128)(2,1)S(1)}, bf16[2048]{0:T(1024)(128)(2,1)}, u32[]{:S(2)}) copy-start(bf16[2048]{0:T(1024)(128)(2,1)} %param.29) | copy-start | bytes 12292
  95.0 4.7 %copy-start.9 = (bf16[2048]{0:T(1024)(128)(2,1)S(1)}, bf16[2048]{0:T(1024)(128)(2,1)}, u32[]{:S(2)}) copy-start(bf16[2048]{0:T(1024)(128)(2,1)} %param.31) | copy-start | bytes 12292
  96.1 20.3 %all-to-all-start.5 = ((bf16[4,280,512]{2,1,0:T(8,128)(2,1)}), bf16[4,280,512]{2,1,0:T(8,128)(2,1)S(1)}, u32[]{:S(2)}, u32[]{:S(2)}) async-start(bf16[4,280,512]{2,1,0:T(8,128)(2,1)} %broadcast_in_dim.40), calls=%async_computation.5 | async-start | bytes 2293760 | tf_op jit(solution)/shard_map/rows/all_to_all | solution.py:18
  116.4 1.0 copy-start.1
  117.4 1.0 copy-start.2
  118.4 1.0 copy-start.3
  139.4 12.5 %copy-start.10 = (f32[24,6]{0,1:T(8,128)S(1)}, f32[24,6]{0,1:T(8,128)}, u32[]{:S(2)}) copy-start(f32[24,6]{0,1:T(8,128)} %param.36) | copy-start | bytes 1732
  139.6 39.0 %copy-start.11 = (bf16[512]{0:T(512)(128)(2,1)S(1)}, bf16[512]{0:T(512)(128)(2,1)}, u32[]{:S(2)}) copy-start(bf16[512]{0:T(512)(128)(2,1)} %param.30) | copy-start | bytes 3076
  140.5 33.8 %all-to-all-start.7 = ((bf16[128,8,128]{2,1,0:T(8,128)(2,1)}), bf16[128,8,128]{2,1,0:T(8,128)(2,1)S(1)}, u32[]{:S(2)}, u32[]{:S(2)}) async-start(bf16[128,8,128]{2,1,0:T(8,128)(2,1)} %reshape.137), calls=%async_computation.7 | async-start | bytes 524288 | tf_op jit(solution)/shard_map/ret/all_to_all | solution.py:18
  175.4 8.4 %all-to-all-start.8 = ((f32[4,1,24]{2,1,0:T(1,128)}), f32[4,1,24]{2,1,0:T(1,128)S(1)}, u32[]{:S(2)}, u32[]{:S(2)}) async-start(f32[4,1,24]{2,1,0:T(1,128)} %broadcast_in_dim.43), calls=%async_computation.8 | async-start | bytes 4096 | tf_op jit(solution)/shard_map/sq/all_to_all | solution.py:18
